TPU v7x, 512 devices: a whole 4x4x16 slice. The times are simulated.
512 devices in a mesh: sp: 64 (over z, y), tp: 8 (over x, core).
Axes of the slice: x: 4, y: 4, z: 16, core: 2. Of those that a mesh axis runs over, the one named last changes fastest.
Arguments:
- skip_stream_entering: bfloat16 [8192, 2048], P(('sp', 'tp')), may hold values from -6 to 6
- content_signal_matrix: bfloat16 [8192, 4096], P('sp', 'tp'), may hold values from -6 to 6
- writer_signal_matrix: bfloat16 [8192, 1024], P('sp', 'tp'), may hold values from -6 to 6
- reader_signal_matrix: bfloat16 [8192, 1024], P('sp', 'tp'), may hold values from -6 to 6
- multiplier_signal: bfloat16 [8192, 4096], P('sp', 'tp'), may hold values from -6 to 6
- interval_before_softplus: float32 [64, 8192], P('tp', 'sp'), may hold values from -7.5 to 0.5
- extra_log_shrink: float32 [64, 8192], P('tp', 'sp'), may hold values from -2.8 to 0
- log_forget_speed: float32 [64], P('tp'), may hold values from -12 to 0
- content_filter_coefs: bfloat16 [4, 4096], P(None, 'tp'), may hold values from -3 to 3
- writer_filter_coefs: bfloat16 [4, 1024], P(None, 'tp'), may hold values from -3 to 3
- reader_filter_coefs: bfloat16 [4, 1024], P(None, 'tp'), may hold values from -3 to 3
- skip_path_factor: float32 [64], P('tp'), may hold values from 0.25 to 2
- cluster_scaling_vector: float32 [4096], P('tp'), may hold values from 0.1 to 1.9
- blend_result_matrix: bfloat16 [4096, 2048], P('tp'), may hold values from -0.09375 to 0.09375
- feature_blend_scaling: float32 [2048], replicated, may hold values from 0.1 to 1.9
- widening_matrix: bfloat16 [2048, 8192], P('sp', 'tp'), may hold values from -0.125 to 0.125
- narrowing_matrix: bfloat16 [8192, 2048], P('tp', 'sp'), may hold values from -0.0625 to 0.0625
Outputs:
- layer_out: bfloat16 [8192, 2048], P(('sp', 'tp'))
All inputs are finite; a program needn't handle non-finite values.
Results may differ from a plain program's by a relative error of at most 0.02.
Values may be sent and summed in bfloat16 or wider, within the bound.
No kernel may reach another device: no remote copies, remote signals or barrier semaphores. Data moves between devices by JAX's collectives and lax.ppermute only.
A program may use at most 64 MiB of HBM per device.

v0:
```python
import jax
import jax.numpy as jnp
from jax import lax
from jax.sharding import Mesh
from jax.sharding import PartitionSpec as P

HEAD_DIM = 64
STATE = 128
BLOCK = 128
SP = ("sp_0", "sp_1")
SP_TP = ("sp_0", "sp_1", "tp")
epsilon = 1e-05


def turned_gather(arrays, axis, dims):
    turned = [jnp.moveaxis(a, dim, 0) for a, dim in zip(arrays, dims)]
    widths = [t[0].size for t in turned]
    both = jnp.concatenate([t.reshape(-1, w) for t, w in zip(turned, widths)], axis=1)
    out = lax.all_gather(both, axis, axis=0, tiled=True)
    blocks = jnp.split(out, [sum(widths[:k]) for k in range(1, len(widths))], axis=1)
    return tuple(
        (
            jnp.moveaxis(b.reshape(-1, *t.shape[1:]), 0, dim)
            for b, t, dim in zip(blocks, turned, dims)
        )
    )


def shifted(value, axis, steps):
    count = lax.axis_size(axis)
    initial, last = (max(0, -steps), min(count, count - steps))
    return lax.ppermute(value, axis, [(source, source + steps) for source in range(initial, last)])


def nothing_yet(value, identity):
    return jax.tree.map(
        lambda part, zero: jnp.zeros_like(part) + jnp.asarray(zero, part.dtype), value, identity
    )


def entering_2(value, axes, combine, identity):
    before = start = nothing_yet(value, identity)
    running = value
    for axis in reversed(axes):
        peers, mine = (lax.axis_size(axis), lax.axis_index(axis))
        pieces = jax.tree.map(
            lambda part, kind: lax.all_gather(part.astype(kind), axis),
            running,
            (jnp.bfloat16, jnp.bfloat16),
        )
        inside, running = (start, start)
        for k in range(peers):
            passed = k < mine
            running = combine(
                running, jax.tree.map(lambda part, own: part[k].astype(own.dtype), pieces, value)
            )
            inside = jax.tree.map(lambda new, old: jnp.where(passed, new, old), running, inside)
        before = combine(inside, before)
    return before


def in_blocks(value, dim, peers):
    dims = value.shape
    blocks = value.reshape(*dims[:dim], peers, dims[dim] // peers, *dims[dim + 1 :])
    return jnp.moveaxis(blocks, dim, 0)


def sum_at_owner(value, axis, dim):
    blocks = in_blocks(value, dim, lax.axis_size(axis))
    arrived = lax.all_to_all(blocks, axis, split_axis=0, concat_axis=0, tiled=True)
    return arrived.astype(jnp.float32).sum(axis=0)


def copy_for_each(value, axis):
    copies = jnp.broadcast_to(value, (lax.axis_size(axis), *value.shape))
    return lax.all_to_all(copies, axis, split_axis=0, concat_axis=0, tiled=True)


def laid_out(blocks, dim):
    dims = list(blocks.shape[1:])
    dims[dim] *= blocks.shape[0]
    return jnp.moveaxis(blocks, 0, dim).reshape(dims)


def gathered_copies(value, axis, dim):
    blocks = copy_for_each(value, axis)
    return laid_out(blocks, dim)


def convolve(inputs, rim_rows, conv_taps):
    width = conv_taps.shape[0]
    length = inputs.shape[0]
    extended = jnp.concatenate([rim_rows, inputs], axis=0)
    summed = extended[0:length].astype(jnp.float32) * conv_taps[0].astype(jnp.float32)
    for offset in range(1, width):
        summed = summed + extended[offset : offset + length].astype(jnp.float32) * conv_taps[
            offset
        ].astype(jnp.float32)
    return jax.nn.silu(summed)


def advance(carried, pair):
    block_state, block_factor = pair
    return (carried * block_factor[..., None, None] + block_state, carried)


def combine_states(earlier, following):
    return (earlier[0] * following[0], earlier[1] * following[0][..., None, None] + following[1])


def blockwise(values, interval_lengths, log_forgetting, key_rows, query_rows):
    length, groups, per_group, width = values.shape
    blocks = length // BLOCK
    value_blocks = values.reshape(blocks, BLOCK, groups, per_group, width)
    step_blocks = jnp.transpose(
        interval_lengths.reshape(groups, per_group, blocks, BLOCK), (2, 3, 0, 1)
    )
    weighted = value_blocks * step_blocks[..., None]
    cumulative = jnp.cumsum(
        jnp.transpose(log_forgetting.reshape(groups, per_group, blocks, BLOCK), (2, 0, 1, 3)),
        axis=-1,
    )
    key_blocks = key_rows.reshape(blocks, BLOCK, groups, -1)
    query_blocks = query_rows.reshape(blocks, BLOCK, groups, -1)
    causal = jnp.tril(jnp.ones((BLOCK, BLOCK), dtype=bool))
    decay_mask = jnp.exp(
        jnp.where(causal, cumulative[..., :, None] - cumulative[..., None, :], -jnp.inf)
    )
    scores = jnp.einsum("clgn,csgn->cgls", query_blocks, key_blocks)
    within = jnp.einsum("cgls,cgrls,csgrp->clgrp", scores, decay_mask, weighted)
    to_end = jnp.exp(cumulative[..., -1:] - cumulative)
    states = jnp.einsum("clgn,cgrl,clgrp->cgrpn", key_blocks, to_end, weighted)
    block_totals = cumulative[..., -1]
    initial = jnp.zeros(states.shape[1:], jnp.float32)
    final, entering = lax.scan(advance, initial, (states, jnp.exp(block_totals)))
    carried = jnp.einsum("clgn,cgrpn,cgrl->clgrp", query_blocks, entering, jnp.exp(cumulative))
    from_start = (jnp.cumsum(block_totals, axis=0) - block_totals)[..., None] + cumulative
    return (within + carried, final, from_start, jnp.sum(block_totals, axis=0))


def normalize(rows, gain):
    widened = rows.astype(jnp.float32)
    scaled = widened * lax.rsqrt(jnp.mean(widened * widened, axis=-1, keepdims=True) + epsilon)
    return (scaled * gain).astype(jnp.bfloat16)


def per_device(
    skip_stream_entering,
    content_signal_matrix,
    writer_signal_matrix,
    reader_signal_matrix,
    multiplier_signal,
    interval_before_softplus,
    extra_log_shrink,
    log_forget_speed,
    content_filter_coefs,
    writer_filter_coefs,
    reader_filter_coefs,
    skip_path_factor,
    cluster_scaling_vector,
    blend_result_matrix,
    feature_blend_scaling,
    widening_matrix,
    narrowing_matrix,
):
    up_whole, down_whole = turned_gather((widening_matrix, narrowing_matrix), SP, (0, 1))
    rim_width = content_filter_coefs.shape[0] - 1
    length = content_signal_matrix.shape[0]
    rims = shifted(
        (
            content_signal_matrix[length - rim_width :],
            writer_signal_matrix[length - rim_width :],
            reader_signal_matrix[length - rim_width :],
        ),
        SP,
        1,
    )
    values = convolve(content_signal_matrix, rims[0], content_filter_coefs)
    key_rows = convolve(writer_signal_matrix, rims[1], writer_filter_coefs)
    query_rows = convolve(reader_signal_matrix, rims[2], reader_filter_coefs)
    local_heads = interval_before_softplus.shape[0]
    local_groups = writer_signal_matrix.shape[1] // STATE
    per_group = local_heads // local_groups
    interval_lengths = jax.nn.softplus(interval_before_softplus)
    log_forgetting = extra_log_shrink - jnp.exp(log_forget_speed)[:, None] * interval_lengths
    shaped = values.reshape(length, local_groups, per_group, HEAD_DIM)
    local_out, end_state, from_start, device_total = blockwise(
        shaped,
        interval_lengths.reshape(local_groups, per_group, length),
        log_forgetting.reshape(local_groups, per_group, length),
        key_rows,
        query_rows,
    )
    identity = (jnp.ones_like(device_total), jnp.zeros_like(end_state))
    incoming = entering_2((jnp.exp(device_total), end_state), SP, combine_states, identity)[1]
    query_blocks = query_rows.reshape(length // BLOCK, BLOCK, local_groups, STATE)
    arriving = jnp.einsum("clgn,grpn,cgrl->clgrp", query_blocks, incoming, jnp.exp(from_start))
    scan_out = (local_out + arriving).reshape(length, local_heads * HEAD_DIM)
    gated = (scan_out + jnp.repeat(skip_path_factor, HEAD_DIM) * values) * jax.nn.silu(
        multiplier_signal.astype(jnp.float32)
    )
    grouped = gated.reshape(length, local_groups, -1)
    grouped = grouped * lax.rsqrt(jnp.mean(grouped * grouped, axis=-1, keepdims=True) + epsilon)
    heads_out = (grouped.reshape(length, -1) * cluster_scaling_vector).astype(jnp.bfloat16)
    mixer_rows = sum_at_owner(
        jnp.dot(heads_out, blend_result_matrix, preferred_element_type=jnp.float32).astype(
            jnp.bfloat16
        ),
        "tp",
        0,
    ).astype(jnp.bfloat16)
    own_rows = (skip_stream_entering.astype(jnp.float32) + mixer_rows.astype(jnp.float32)).astype(
        jnp.bfloat16
    )
    normed_all = gathered_copies(normalize(own_rows, feature_blend_scaling), "tp", 0)
    lifted = jnp.dot(normed_all, up_whole, preferred_element_type=jnp.float32)
    lifted = jax.nn.relu(lifted)
    hidden = (lifted * lifted).astype(jnp.bfloat16)
    mlp_rows = sum_at_owner(
        jnp.dot(hidden, down_whole, preferred_element_type=jnp.float32).astype(jnp.bfloat16),
        "tp",
        0,
    ).astype(jnp.bfloat16)
    return (own_rows.astype(jnp.float32) + mlp_rows.astype(jnp.float32)).astype(jnp.bfloat16)


def solution(mesh):
    torus = Mesh(mesh.devices.reshape(16, 4, mesh.shape["tp"]), ("sp_0", "sp_1", "tp"))
    placed = (
        P(SP_TP, None),
        P(SP, "tp"),
        P(SP, "tp"),
        P(SP, "tp"),
        P(SP, "tp"),
        P("tp", SP),
        P("tp", SP),
        P("tp"),
        P(None, "tp"),
        P(None, "tp"),
        P(None, "tp"),
        P("tp"),
        P("tp"),
        P("tp", None),
        P(),
        P(SP, "tp"),
        P("tp", SP),
    )
    return jax.shard_map(
        per_device, mesh=torus, in_specs=placed, out_specs=P(SP_TP, None), check_vma=False
    )
```

profile of v0, /device:TPU:1, one launch (start us, length us, event | category | flops | bytes accessed | tf_op | source)
XLA Modules:
  0.0 304.0 jit_solution(4290324773650001404)
XLA Ops:
  6.5 0.0 copy-start
  6.5 0.0 all-gather.5.cloned.1.call-start
  6.5 0.9 slice.212
  7.4 0.2 copy.24
  7.6 4.0 %collective-permute-start.2 = (bf16[3,512]{0,1:T(8,128)(2,1)S(1)}, bf16[3,512]{0,1:T(8,128)(2,1)S(1)}, u32[]{:S(2)}, u32[]{:S(2)}) collective-permute-start(bf16[3,512]{0,1:T(8,128)(2,1)S(1)} %copy.24), channel_id=1, source_target_pairs={{0,8},{8,16},{16,24},{24,32},{32,40},{40,48},{48,56},{56,64},{64,7... | collective-permute-start | bytes 9224 | tf_op jit(solution)/shard_map/ppermute | solution.py:32
  11.6 0.7 slice.204
  12.3 3.2 %collective-permute-start.1 = (bf16[3,128]{1,0:T(4,128)(2,1)S(1)}, bf16[3,128]{1,0:T(4,128)(2,1)S(1)}, u32[]{:S(2)}, u32[]{:S(2)}) collective-permute-start(bf16[3,128]{1,0:T(4,128)(2,1)S(1)} %slice.204), channel_id=1, source_target_pairs={{0,8},{8,16},{16,24},{24,32},{32,40},{40,48},{48,56},{56,64},{64,7... | collective-permute-start | bytes 2312 | tf_op jit(solution)/shard_map/ppermute | solution.py:32
  15.5 0.7 exp.73
  16.2 0.8 fusion.190
  16.9 0.3 reduce_window_sum.17
  17.2 0.2 subtract_reduce_fusion
  17.4 0.1 slice_exponential_fusion
  17.5 0.9 slice_convert_fusion.3
  18.3 0.8 bitcast_convert_fusion.3
  19.2 0.1 copy.27
  19.3 8.0 %all-gather = bf16[4,1,8,1]{2,3,1,0:T(2,128)(2,1)S(1)} all-gather(bf16[1,1,8,1]{2,3,1,0:T(2,128)(2,1)S(1)} %copy.27), channel_id=2, replica_groups=mesh['sp_0'=16,'sp_1'=4,'tp'=8] {'sp_1'}, dimensions={0}, use_global_device_ids=true | all-gather | bytes 80 | tf_op jit(solution)/shard_map/all_gather | solution.py:47
  27.2 0.1 exponential_bitcast_fusion.2
  27.3 1.0 copy.25
  28.3 0.0 collective-permute-done.1
  28.3 1.0 divide_multiply_fusion.1
  29.3 0.0 collective-permute-done.2
  29.3 0.5 divide_multiply_fusion
  29.9 0.2 fusion.22
  30.0 11.4 %all-gather.1 = bf16[32,64,128]{2,1,0:T(8,128)(2,1)S(1)} all-gather(bf16[8,64,128]{2,1,0:T(8,128)(2,1)S(1)} %fusion.22), channel_id=3, replica_groups=mesh['sp_0'=16,'sp_1'=4,'tp'=8] {'sp_1'}, dimensions={0}, use_global_device_ids=true | all-gather | bytes 655360 | tf_op jit(solution)/shard_map/all_gather | solution.py:47
  41.4 0.9 fusion.104
  42.3 0.0 all-gather.5.cloned.1.call-update
  42.3 0.0 all-gather.7.cloned.1.call-start
  42.4 1.6 pad_maximum_fusion.1
  43.9 0.0 all-gather.7.cloned.1.call-update
  43.9 0.7 slice.196
  44.6 1.3 collective-permute-start
  45.9 27.0 %all_gather.22 = bf16[16,1,8]{2,1,0:T(2,128)(2,1)S(1)} all-gather(bf16[1,1,8]{2,1,0:T(2,128)(2,1)S(1)} %convert_bitcast_fusion), channel_id=1, replica_groups=mesh['sp_0'=16,'sp_1'=4,'tp'=8] {'sp_0'}, dimensions={0}, use_global_device_ids=true | all-gather | bytes 272 | tf_op jit(solution)/shard_map/all_gather | solution.py:47
  73.0 0.8 bitcast_convert_fusion.7
  73.8 1.0 copy.28
  74.9 0.7 broadcast_in_dim.20
  75.6 0.1 mul.651
  75.7 0.0 collective-permute-done
  75.7 1.0 divide_multiply_fusion.2
  76.6 0.2 fusion.19
  76.8 0.2 fusion.216
  77.0 34.8 %all-gather.5.cloned.1.call-done = bf16[16,1,8,64,128]{4,3,2,1,0:T(8,128)(2,1)} async-done(((bf16[1,1,8,64,128]{4,3,2,1,0:T(8,128)(2,1)}), bf16[16,1,8,64,128]{4,3,2,1,0:T(8,128)(2,1)}) %all-gather.5.cloned.1.call-update) | async-done | bytes 2097168 | tf_op jit(solution)/shard_map/all_gather | solution.py:47
  111.8 0.0 copy-start.3
  111.8 2.5 fusion.18
  114.3 0.0 copy-start.1
  114.3 0.0 copy-start.2
  114.4 0.4 fusion.21
  114.7 0.2 multiply_reduce_fusion
  114.9 0.0 copy-done
  114.9 0.0 copy-done.3
  114.9 0.6 convolution_convert_fusion
  115.5 23.3 %all_to_all.15 = bf16[8,16,2048]{2,1,0:T(8,128)(2,1)S(1)} all-to-all(bf16[8,16,2048]{2,1,0:T(8,128)(2,1)S(1)} %bitcast.221), channel_id=1, replica_groups=mesh['sp_0'=16,'sp_1'=4,'tp'=8] {'tp'}, dimensions={0} | all-to-all | bytes 1048576 | tf_op jit(solution)/shard_map/all_to_all | solution.py:70
  138.8 0.1 reduce_sum.47
  138.9 0.0 copy-done.1
  138.9 0.1 fusion.113
  139.0 0.0 copy-done.2
  139.0 0.1 fusion.115
  139.2 12.8 %all_to_all.16 = bf16[8,16,2048]{2,1,0:T(8,128)(2,1)S(1)} all-to-all(bf16[8,16,2048]{2,1,0:T(8,128)(2,1)S(1)} %broadcast_in_dim.21), channel_id=1, replica_groups=mesh['sp_0'=16,'sp_1'=4,'tp'=8] {'tp'}, dimensions={0} | all-to-all | bytes 1048576 | tf_op jit(solution)/shard_map/all_to_all | solution.py:76
  151.9 117.2 %all-gather.7.cloned.1.call-done = bf16[2048,2048]{1,0:T(8,128)(2,1)} async-done(((bf16[32,2048]{1,0:T(8,128)(2,1)}), bf16[2048,2048]{1,0:T(8,128)(2,1)}) %all-gather.7.cloned.1.call-update) | async-done | bytes 8388624 | tf_op jit(solution)/shard_map/all_gather | solution.py:19
  269.1 5.6 %fusion.4 = bf16[128,2048]{1,0:T(8,128)(2,1)S(1)} fusion(bf16[2048,2048]{1,0:T(8,128)(2,1)} %all-gather.7.cloned.1.call-done, bf16[128,2048]{1,0:T(8,128)(2,1)S(1)} %bitcast.222), kind=kOutput, calls=%fused_computation.4 | convolution fusion | flops 1074397184 | bytes 9437184 | tf_op jit(solution)/shard_map/dot_general | solution.py:220
  274.7 21.8 %all_to_all.17 = bf16[8,16,2048]{2,1,0:T(8,128)(2,1)S(1)} all-to-all(bf16[8,16,2048]{2,1,0:T(8,128)(2,1)S(1)} %bitcast.223), channel_id=1, replica_groups=mesh['sp_0'=16,'sp_1'=4,'tp'=8] {'tp'}, dimensions={0} | all-to-all | bytes 1048576 | tf_op jit(solution)/shard_map/all_to_all | solution.py:70
  296.5 0.1 reduce_sum.49
  296.5 0.7 fusion.116
  (10 shorter events, 0.1 us)
Async XLA Ops:
  6.5 108.4 %copy-start = (bf16[512,2048]{1,0:T(8,128)(2,1)S(1)}, bf16[512,2048]{1,0:T(8,128)(2,1)}, u32[]{:S(2)}) copy-start(bf16[512,2048]{1,0:T(8,128)(2,1)} %param.30) | copy-start | bytes 6291460
  6.5 105.3 %all-gather.5.cloned.1.call-start = ((), (), s32[]{:S(2)}) async-start(), calls=%async_computation.3 | async-start | bytes 2228224 | tf_op jit(solution)/shard_map/all_gather | solution.py:47
  7.6 21.8 %collective-permute-start.2 = (bf16[3,512]{0,1:T(8,128)(2,1)S(1)}, bf16[3,512]{0,1:T(8,128)(2,1)S(1)}, u32[]{:S(2)}, u32[]{:S(2)}) collective-permute-start(bf16[3,512]{0,1:T(8,128)(2,1)S(1)} %copy.24), channel_id=1, source_target_pairs={{0,8},{8,16},{16,24},{24,32},{32,40},{40,48},{48,56},{56,64},{64,7... | collective-permute-start | bytes 9224 | tf_op jit(solution)/shard_map/ppermute | solution.py:32
  12.3 16.0 %collective-permute-start.1 = (bf16[3,128]{1,0:T(4,128)(2,1)S(1)}, bf16[3,128]{1,0:T(4,128)(2,1)S(1)}, u32[]{:S(2)}, u32[]{:S(2)}) collective-permute-start(bf16[3,128]{1,0:T(4,128)(2,1)S(1)} %slice.204), channel_id=1, source_target_pairs={{0,8},{8,16},{16,24},{24,32},{32,40},{40,48},{48,56},{56,64},{64,7... | collective-permute-start | bytes 2312 | tf_op jit(solution)/shard_map/ppermute | solution.py:32
  42.3 226.8 %all-gather.7.cloned.1.call-start = ((), (), s32[]{:S(2)}) async-start(), calls=%async_computation.4 | async-start | bytes 8519680 | tf_op jit(solution)/shard_map/all_gather | solution.py:19
  44.6 31.1 %collective-permute-start = (bf16[3,128]{1,0:T(4,128)(2,1)S(1)}, bf16[3,128]{1,0:T(4,128)(2,1)S(1)}, u32[]{:S(2)}, u32[]{:S(2)}) collective-permute-start(bf16[3,128]{1,0:T(4,128)(2,1)S(1)} %slice.196), channel_id=1, source_target_pairs={{0,8},{8,16},{16,24},{24,32},{32,40},{40,48},{48,56},{56,64},{64,7... | collective-permute-start | bytes 2312 | tf_op jit(solution)/shard_map/ppermute | solution.py:32
  111.8 3.1 %copy-start.3 = (f32[512]{0:T(512)S(1)}, f32[512]{0:T(512)}, u32[]{:S(2)}) copy-start(f32[512]{0:T(512)} %param.29) | copy-start | bytes 6148
  114.3 24.5 %copy-start.1 = (bf16[16,2048]{1,0:T(8,128)(2,1)S(1)}, bf16[16,2048]{1,0:T(8,128)(2,1)}, u32[]{:S(2)}) copy-start(bf16[16,2048]{1,0:T(8,128)(2,1)} %param.17) | copy-start | bytes 196612
  114.3 24.7 %copy-start.2 = (f32[2048]{0:T(1024)S(1)}, f32[2048]{0:T(1024)}, u32[]{:S(2)}) copy-start(f32[2048]{0:T(1024)} %param.31) | copy-start | bytes 24580
Sparse Core Ops, SparseCore 0:
  42.4 69.3 all-gather.4
  114.8 154.2 all-gather.6
where the time goes:
time: 305 us; the launch traced here: 304 us
  waiting for transfers between devices  152 us (50%)
  blocking collectives  104 us (34%)
  between operations  13.7 us (4%)
  other arithmetic  10.1 us (3%)
  matrix products  9.51 us (3%)
  starting transfers between devices  8.53 us (3%)
  local copies, waits for them, and re-layouts  6.08 us (2%)
    all_gather x1, waiting for transfers between devices, turned_gather(): out = lax.all_gather(both, axis, axis=0, tiled=True)  117 us
    all_gather x3, blocking collectives, entering_2(): lax.all_gather(part.astype(kind), axis)  46.3 us
    all_to_all x2, blocking collectives, sum_at_owner(): lax.all_to_all(blocks, axis, split_axis=0, concat_axis=0, tiled=True)  45.1 us
    all_gather x1, waiting for transfers between devices, entering_2(): lax.all_gather(part.astype(kind), axis)  34.8 us
    all_to_all x1, blocking collectives, copy_for_each(): return lax.all_to_all(copies, axis, split_axis=0, concat_axis=0, tiled=True)  12.8 us
    ppermute x3, starting transfers between devices, shifted(): lax.ppermute(value, axis, [(source, source + steps) for source in range(i...  8.49 us
  transfers between devices with their start and end apart: 5, of which 2 were waited for; matrix products, arithmetic and copies ran while one was open for 6% of the time, Pallas kernels for 0%

commit v1 on v0

--- a/solution.py
+++ b/solution.py
@@ -16,7 +16,7 @@
     turned = [jnp.moveaxis(a, dim, 0) for a, dim in zip(arrays, dims)]
     widths = [t[0].size for t in turned]
     both = jnp.concatenate([t.reshape(-1, w) for t, w in zip(turned, widths)], axis=1)
-    out = lax.all_gather(both, axis, axis=0, tiled=True)
+    out = jnp.concatenate(lax.all_to_all(jnp.stack([both] * lax.psum(1, axis)), axis, 0, 0), axis=0)
     blocks = jnp.split(out, [sum(widths[:k]) for k in range(1, len(widths))], axis=1)
     return tuple(
         (

time: 305 us -> 562 us (1.84)
  blocking collectives: 104 us -> 463 us
  waiting for transfers between devices: 152 us -> 46.3 us
    all_to_all x1, blocking collectives: 12.8 us -> 376 us  [turned_gather(): lax.all_to_all(jnp.stack([both] * lax.psum(1, axis)), axis, 0, 0)]
    all_gather x1 -> x0, waiting for transfers between devices: 117 us -> none  [turned_gather(): out = lax.all_gather(both, axis, axis=0, tiled=True)]
    all_to_all x0 -> x1, waiting for transfers between devices: none -> 9.35 us  [copy_for_each(): return lax.all_to_all(copies, axis, split_axis=0, concat_axis=0, tiled=True)]
  transfers between devices with their start and end apart: 5 -> 5, of which waited for: 2 -> 2; matrix products, arithmetic and copies ran while one was open for 6% -> 2% of each run, Pallas kernels for 0% -> 0%
where the time goes in v1:
time: 562 us
  blocking collectives  463 us (82%)
  waiting for transfers between devices  46.3 us (8%)
  between operations  13.7 us (2%)
  starting transfers between devices  12.9 us (2%)
  matrix products  9.48 us (2%)
  other arithmetic  8.51 us (2%)
  local copies, waits for them, and re-layouts  7.94 us (1%)
    all_to_all x1, blocking collectives, turned_gather(): lax.all_to_all(jnp.stack([both] * lax.psum(1, axis)), axis, 0, 0)  376 us
    all_gather x3, blocking collectives, entering_2(): lax.all_gather(part.astype(kind), axis)  46.1 us
    all_to_all x2, blocking collectives, sum_at_owner(): lax.all_to_all(blocks, axis, split_axis=0, concat_axis=0, tiled=True)  41.2 us
    all_gather x1, waiting for transfers between devices, entering_2(): lax.all_gather(part.astype(kind), axis)  36.9 us
  transfers between devices with their start and end apart: 5, of which 2 were waited for; matrix products, arithmetic and copies ran while one was open for 2% of the time, Pallas kernels for 0%

profile of v1, /device:TPU:1, one launch (start us, length us, event | category | flops | bytes accessed | tf_op | source)
XLA Modules:
  0.0 561.6 jit_solution(11087689786327529356)
XLA Ops:
  6.5 0.0 copy-start
  6.5 0.0 all-gather.4.cloned.1.call-start
  6.5 0.9 slice.212
  7.4 0.2 copy.24
  7.6 4.0 collective-permute-start.2
  11.6 0.7 slice.204
  12.3 3.2 collective-permute-start.1
  15.5 0.7 exp.73
  16.2 0.8 fusion.190
  16.9 0.3 reduce_window_sum.17
  17.2 0.1 slice_exponential_fusion
  17.3 0.2 subtract_reduce_fusion
  17.5 0.8 slice_convert_fusion.3
  18.3 0.1 copy.27
  18.4 8.0 %all-gather = bf16[4,1,8,1]{2,3,1,0:T(2,128)(2,1)S(1)} all-gather(bf16[1,1,8,1]{2,3,1,0:T(2,128)(2,1)S(1)} %copy.27), channel_id=2, replica_groups=mesh['sp_0'=16,'sp_1'=4,'tp'=8] {'sp_1'}, dimensions={0}, use_global_device_ids=true | all-gather | bytes 80 | tf_op jit(solution)/shard_map/all_gather | solution.py:47
  26.4 0.8 bitcast_convert_fusion.3
  27.2 0.1 exponential_bitcast_fusion.2
  27.3 1.0 copy.25
  28.3 0.0 collective-permute-done.1
  28.3 1.0 divide_multiply_fusion.1
  29.3 0.0 collective-permute-done.2
  29.3 0.5 divide_multiply_fusion
  29.9 0.2 fusion.22
  30.0 11.4 %all-gather.1 = bf16[32,64,128]{2,1,0:T(8,128)(2,1)S(1)} all-gather(bf16[8,64,128]{2,1,0:T(8,128)(2,1)S(1)} %fusion.22), channel_id=3, replica_groups=mesh['sp_0'=16,'sp_1'=4,'tp'=8] {'sp_1'}, dimensions={0}, use_global_device_ids=true | all-gather | bytes 655360 | tf_op jit(solution)/shard_map/all_gather | solution.py:47
  41.4 0.8 fusion.104
  42.3 0.0 all-gather.4.cloned.1.call-update
  42.3 0.7 slice.196
  43.0 1.3 collective-permute-start
  44.3 1.0 copy.28
  45.3 0.7 broadcast_in_dim.20
  46.0 0.1 mul.651
  46.1 26.8 %all_gather.19 = bf16[16,1,8]{2,1,0:T(2,128)(2,1)S(1)} all-gather(bf16[1,1,8]{2,1,0:T(2,128)(2,1)S(1)} %convert_bitcast_fusion), channel_id=1, replica_groups=mesh['sp_0'=16,'sp_1'=4,'tp'=8] {'sp_0'}, dimensions={0}, use_global_device_ids=true | all-gather | bytes 272 | tf_op jit(solution)/shard_map/all_gather | solution.py:47
  72.9 0.8 bitcast_convert_fusion.7
  73.8 0.0 collective-permute-done
  73.8 1.0 divide_multiply_fusion.2
  74.8 0.2 fusion.19
  75.0 0.1 fusion.216
  75.1 36.9 %all-gather.4.cloned.1.call-done = bf16[16,1,8,64,128]{4,3,2,1,0:T(8,128)(2,1)} async-done(((bf16[1,1,8,64,128]{4,3,2,1,0:T(8,128)(2,1)}), bf16[16,1,8,64,128]{4,3,2,1,0:T(8,128)(2,1)}) %all-gather.4.cloned.1.call-update) | async-done | bytes 2097168 | tf_op jit(solution)/shard_map/all_gather | solution.py:47
  112.0 2.5 fusion.18
  114.5 0.0 copy-start.1
  114.5 0.0 copy-start.4
  114.5 0.0 copy-start.2
  114.6 0.0 copy-start.3
  114.6 0.4 fusion.21
  114.9 0.2 multiply_reduce_fusion
  115.1 0.0 copy-done
  115.1 0.0 copy-done.5
  115.1 0.6 convolution_convert_fusion
  115.7 23.0 %all_to_all.20 = bf16[8,16,2048]{2,1,0:T(8,128)(2,1)S(1)} all-to-all(bf16[8,16,2048]{2,1,0:T(8,128)(2,1)S(1)} %bitcast.223), channel_id=1, replica_groups=mesh['sp_0'=16,'sp_1'=4,'tp'=8] {'tp'}, dimensions={0} | all-to-all | bytes 1048576 | tf_op jit(solution)/shard_map/all_to_all | solution.py:70
  138.7 0.1 reduce_sum.47
  138.8 0.0 copy-done.1
  138.8 0.1 fusion.113
  138.9 0.0 copy-done.4
  138.9 0.1 fusion.115
  139.0 0.8 broadcast_in_dim.21
  139.9 4.4 all-to-all-start.1
  144.3 0.0 copy-done.2
  144.3 9.4 %all-to-all-done.1 = bf16[8,16,2048]{2,1,0:T(8,128)(2,1)S(1)} async-done(((bf16[8,16,2048]{2,1,0:T(8,128)(2,1)}), bf16[8,16,2048]{2,1,0:T(8,128)(2,1)S(1)}, u32[]{:S(2)}, u32[]{:S(2)}) %all-to-all-start.1) | async-done | bytes 524320 | tf_op jit(solution)/shard_map/all_to_all | solution.py:76
  153.7 1.1 stack.2
  154.7 375.5 %all_to_all.21 = bf16[64,32,2048]{2,1,0:T(8,128)(2,1)} all-to-all(bf16[64,32,2048]{2,1,0:T(8,128)(2,1)S(1)} %stack.2), channel_id=1, replica_groups=mesh['sp_0'=16,'sp_1'=4,'tp'=8] {'sp_0','sp_1'}, dimensions={0} | all-to-all | bytes 16777216 | tf_op jit(solution)/shard_map/all_to_all | solution.py:19
  530.3 5.6 fusion.4
  535.8 18.2 %all_to_all.22 = bf16[8,16,2048]{2,1,0:T(8,128)(2,1)S(1)} all-to-all(bf16[8,16,2048]{2,1,0:T(8,128)(2,1)S(1)} %bitcast.225), channel_id=1, replica_groups=mesh['sp_0'=16,'sp_1'=4,'tp'=8] {'tp'}, dimensions={0} | all-to-all | bytes 1048576 | tf_op jit(solution)/shard_map/all_to_all | solution.py:70
  554.0 0.1 reduce_sum.49
  554.1 0.7 fusion.116
  (12 shorter events, 0.1 us)
Async XLA Ops:
  6.5 108.6 %copy-start = (bf16[512,2048]{1,0:T(8,128)(2,1)S(1)}, bf16[512,2048]{1,0:T(8,128)(2,1)}, u32[]{:S(2)}) copy-start(bf16[512,2048]{1,0:T(8,128)(2,1)} %param.30) | copy-start | bytes 6291460
  6.5 105.5 %all-gather.4.cloned.1.call-start = ((), (), s32[]{:S(2)}) async-start(), calls=%async_computation.4 | async-start | bytes 2228224 | tf_op jit(solution)/shard_map/all_gather | solution.py:47
  7.6 21.8 %collective-permute-start.2 = (bf16[3,512]{0,1:T(8,128)(2,1)S(1)}, bf16[3,512]{0,1:T(8,128)(2,1)S(1)}, u32[]{:S(2)}, u32[]{:S(2)}) collective-permute-start(bf16[3,512]{0,1:T(8,128)(2,1)S(1)} %copy.24), channel_id=1, source_target_pairs={{0,8},{8,16},{16,24},{24,32},{32,40},{40,48},{48,56},{56,64},{64,7... | collective-permute-start | bytes 9224 | tf_op jit(solution)/shard_map/ppermute | solution.py:32
  12.3 16.0 %collective-permute-start.1 = (bf16[3,128]{1,0:T(4,128)(2,1)S(1)}, bf16[3,128]{1,0:T(4,128)(2,1)S(1)}, u32[]{:S(2)}, u32[]{:S(2)}) collective-permute-start(bf16[3,128]{1,0:T(4,128)(2,1)S(1)} %slice.204), channel_id=1, source_target_pairs={{0,8},{8,16},{16,24},{24,32},{32,40},{40,48},{48,56},{56,64},{64,7... | collective-permute-start | bytes 2312 | tf_op jit(solution)/shard_map/ppermute | solution.py:32
  43.0 30.8 %collective-permute-start = (bf16[3,128]{1,0:T(4,128)(2,1)S(1)}, bf16[3,128]{1,0:T(4,128)(2,1)S(1)}, u32[]{:S(2)}, u32[]{:S(2)}) collective-permute-start(bf16[3,128]{1,0:T(4,128)(2,1)S(1)} %slice.196), channel_id=1, source_target_pairs={{0,8},{8,16},{16,24},{24,32},{32,40},{40,48},{48,56},{56,64},{64,7... | collective-permute-start | bytes 2312 | tf_op jit(solution)/shard_map/ppermute | solution.py:32
  112.0 3.1 copy-start.5
  114.5 24.2 %copy-start.1 = (bf16[16,2048]{1,0:T(8,128)(2,1)S(1)}, bf16[16,2048]{1,0:T(8,128)(2,1)}, u32[]{:S(2)}) copy-start(bf16[16,2048]{1,0:T(8,128)(2,1)} %param.17) | copy-start | bytes 196612
  114.5 24.4 %copy-start.4 = (f32[2048]{0:T(1024)S(1)}, f32[2048]{0:T(1024)}, u32[]{:S(2)}) copy-start(f32[2048]{0:T(1024)} %param.31) | copy-start | bytes 24580
  114.5 29.7 %copy-start.2 = (bf16[1024,32]{0,1:T(8,128)(2,1)S(1)}, bf16[1024,32]{0,1:T(8,128)(2,1)}, u32[]{:S(2)}) copy-start(bf16[1024,32]{0,1:T(8,128)(2,1)} %param.33) | copy-start | bytes 196612
  114.6 29.7 %copy-start.3 = (bf16[32,1024]{1,0:T(8,128)(2,1)S(1)}, bf16[32,1024]{1,0:T(8,128)(2,1)}, u32[]{:S(2)}) copy-start(bf16[32,1024]{1,0:T(8,128)(2,1)} %param.32) | copy-start | bytes 196612
  139.9 13.8 %all-to-all-start.1 = ((bf16[8,16,2048]{2,1,0:T(8,128)(2,1)}), bf16[8,16,2048]{2,1,0:T(8,128)(2,1)S(1)}, u32[]{:S(2)}, u32[]{:S(2)}) async-start(bf16[8,16,2048]{2,1,0:T(8,128)(2,1)} %broadcast_in_dim.21), calls=%async_computation.1 | async-start | bytes 1048576 | tf_op jit(solution)/shard_map/all_to_all | solution.py:76
Sparse Core Ops, SparseCore 0:
  42.4 69.5 all-gather.3
